TPU v7x, 32 devices: a whole 2x2x4 slice. The times are simulated.
32 devices in a mesh: sp: 8 (over z, y), tp: 4 (over x, core).
Axes of the slice: x: 2, y: 2, z: 4, core: 2. Of those that a mesh axis runs over, the one named last changes fastest.
Arguments:
- stream: bfloat16 [4096, 2048], P('sp', 'tp'), may hold values from -6 to 6
- doc_ids: int32 [4096], P('sp'), may hold values from 0 to 3, never falling along the last dimension, each value on 1 to 2304 neighbouring positions
- norm_gain: float32 [2, 2048], replicated, may hold values from 0.1 to 1.9
- gate_proj: bfloat16 [2, 2048, 2048], P(None, 'sp', 'tp'), may hold values from -0.125 to 0.125
- input_gate: bfloat16 [2, 2048, 2048], P(None, 'sp', 'tp'), may hold values from -0.125 to 0.125
- value_proj: bfloat16 [2, 2048, 2048], P(None, 'sp', 'tp'), may hold values from -0.125 to 0.125
- taps: float32 [2, 3, 2048], P(None, None, 'tp'), may hold values from -3 to 3
- out_proj: bfloat16 [2, 2048, 2048], P(None, 'tp', 'sp'), may hold values from -0.125 to 0.125
Outputs:
- result: bfloat16 [4096, 2048], P('sp', 'tp')
Inputs may be any that keep to these rules, and one draw needn't show every extreme that they name: `doc_ids`: document numbers never fall along the sequence; each document holds 1 to 2304 positions.
All inputs are finite; a program needn't handle non-finite values.
Results may differ from a plain program's by a relative error of at most 0.03.
Values may be sent and summed in bfloat16 or wider, within the bound.
A program may use at most 64 MiB of HBM per device.

v0:
```python
import jax
import jax.numpy as jnp
from jax import lax
from jax.sharding import PartitionSpec as P

epsilon = 1e-06


def with_halo(value, sides, width):
    for axis, dim in sides:
        size, length = (lax.axis_size(axis), value.shape[dim])
        up = [(i, (i + 1) % size) for i in range(size - 1)]
        down = [(j, i) for i, j in up]
        last = lax.slice_in_dim(value, length - width, length, axis=dim)
        leading = lax.slice_in_dim(value, 0, width, axis=dim)
        before = lax.ppermute(last, axis, up)
        after = lax.ppermute(leading, axis, down)
        value = jnp.concatenate([before, value, after], axis=dim)
    return value


def per_device(stream, doc_ids, norm_gain, gate_proj, input_gate, value_proj, taps, out_proj):
    layers = gate_proj.shape[0]
    gathered_in = (
        lax.all_gather(gate_proj, "sp", axis=1, tiled=True),
        lax.all_gather(input_gate, "sp", axis=1, tiled=True),
        lax.all_gather(value_proj, "sp", axis=1, tiled=True),
    )
    gathered_out = lax.all_gather(out_proj, "sp", axis=2, tiled=True)
    current = stream
    for layer_index in range(layers):
        full_rows = lax.all_gather(current, "tp", axis=1, tiled=True)
        widened = full_rows.astype(jnp.float32)
        scale = lax.rsqrt(jnp.mean(widened * widened, axis=-1, keepdims=True) + epsilon)
        normed = (widened * scale * norm_gain[layer_index]).astype(jnp.bfloat16)
        gate_b = jnp.dot(normed, gathered_in[0][layer_index], preferred_element_type=jnp.float32)
        gate_c = jnp.dot(normed, gathered_in[1][layer_index], preferred_element_type=jnp.float32)
        values = jnp.dot(normed, gathered_in[2][layer_index], preferred_element_type=jnp.float32)
        gate_b = gate_b.astype(jnp.bfloat16)
        gate_c = gate_c.astype(jnp.bfloat16)
        values = values.astype(jnp.bfloat16)
        mixed_in = (gate_c.astype(jnp.float32) * values.astype(jnp.float32)).astype(jnp.bfloat16)
        padded, doc_padded = (
            with_halo(mixed_in, (("sp", 0),), 1),
            with_halo(doc_ids, (("sp", 0),), 1),
        )
        same_prev = (doc_padded[:-2] == doc_ids)[:, None]
        same_next = (doc_padded[2:] == doc_ids)[:, None]
        kernel_taps = taps[layer_index]
        convolved = (
            jnp.where(same_prev, kernel_taps[0] * padded[:-2].astype(jnp.float32), 0.0)
            + kernel_taps[1] * mixed_in.astype(jnp.float32)
            + jnp.where(same_next, kernel_taps[2] * padded[2:].astype(jnp.float32), 0.0)
        )
        gated = (gate_b.astype(jnp.float32) * convolved).astype(jnp.bfloat16)
        partials = jnp.dot(gated, gathered_out[layer_index], preferred_element_type=jnp.float32)
        summed = lax.psum_scatter(
            partials.astype(jnp.bfloat16), "tp", scatter_dimension=1, tiled=True
        ).astype(jnp.float32)
        current = (current.astype(jnp.float32) + summed).astype(jnp.bfloat16)
    return current


def solution(mesh):
    in_specs = (
        P("sp", "tp"),
        P("sp"),
        P(),
        P(None, "sp", "tp"),
        P(None, "sp", "tp"),
        P(None, "sp", "tp"),
        P(None, None, "tp"),
        P(None, "tp", "sp"),
    )
    out_specs = P("sp", "tp")
    return jax.shard_map(
        per_device, mesh=mesh, in_specs=in_specs, out_specs=out_specs, check_vma=False
    )
```

profile of v0, /device:TPU:0, one launch (start us, length us, event | category | flops | bytes accessed | tf_op | source)
XLA Modules:
  0.0 454.6 jit_solution(15519410524372381653)
XLA Ops:
  6.5 0.0 all-gather.7.cloned.1.call-start
  6.5 0.7 all-gather.7.cloned.1.call-update
  7.3 0.0 all-gather.13.cloned.1.call-start
  7.3 0.7 all-gather.13.cloned.1.call-update
  8.0 0.0 all-gather.11.cloned.1.call-start
  8.1 0.7 all-gather.11.cloned.1.call-update
  8.7 0.0 all-gather.9.cloned.1.call-start
  8.8 0.5 all-gather.9.cloned.1.call-update
  9.3 0.0 all-gather.15.cloned.1.call-start
  9.4 0.5 all-gather.15.cloned.1.call-update
  9.9 0.0 reduce-scatter.3.cloned.1.call-start
  9.9 1.3 fusion.64
  11.3 5.4 %collective-permute-start = (s32[1]{0:T(128)}, s32[1]{0:T(128)}, u32[]{:S(2)}, u32[]{:S(2)}) collective-permute-start(s32[1]{0:T(128)} %get-tuple-element.21), channel_id=1, source_target_pairs={{0,4},{4,8},{8,12},{12,16},{16,20},{20,24},{24,28},{1,5},{5,9},{9,... | collective-permute-start | bytes 20 | tf_op jit(solution)/shard_map/ppermute | solution.py:16
  16.7 1.3 collective-permute-start.2
  18.0 0.8 fusion.63
  18.8 0.8 fusion.62
  19.6 0.0 collective-permute-done
  19.6 2.5 collective-permute-done.2
  22.2 2.1 pad_add_fusion
  24.3 9.9 %all-gather.7.cloned.1.call-done = bf16[512,2048]{1,0:T(8,128)(2,1)} async-done(((bf16[512,512]{1,0:T(8,128)(2,1)}), bf16[512,2048]{1,0:T(8,128)(2,1)}) %all-gather.7.cloned.1.call-update) | async-done | bytes 2097168 | tf_op jit(solution)/shard_map/all_gather | solution.py:32
  34.2 2.1 fusion
  36.3 72.9 %all-gather.13.cloned.1.call-done = bf16[2,2048,512]{2,1,0:T(8,128)(2,1)} async-done(((bf16[2,256,512]{2,1,0:T(8,128)(2,1)}), bf16[2,2048,512]{2,1,0:T(8,128)(2,1)}) %all-gather.13.cloned.1.call-update) | async-done | bytes 4194320 | tf_op jit(solution)/shard_map/all_gather | solution.py:27
  109.2 0.0 copy-start.2
  109.2 4.7 %fusion.19 = f32[512,512]{1,0:T(8,128)} fusion(bf16[2,2048,512]{2,1,0:T(8,128)(2,1)} %all-gather.13.cloned.1.call-done, bf16[512,2048]{1,0:T(8,128)(2,1)} %all-gather.7.cloned.1.call-done, f32[2048]{0:T(1024)S(1)} %bitcast.79, f32[512]{0:T(512)S(1)} %add_rsqrt_fusion.1), kind=kOutput, calls=%fused_computation.33 | convolution fusion | flops 1078460416 | bytes 5253120 | tf_op jit(solution)/shard_map/dot_general | solution.py:38
  113.9 0.0 copy-start.4
  113.9 68.9 %all-gather.11.cloned.1.call-done = bf16[2,2048,512]{2,1,0:T(8,128)(2,1)} async-done(((bf16[2,256,512]{2,1,0:T(8,128)(2,1)}), bf16[2,2048,512]{2,1,0:T(8,128)(2,1)}) %all-gather.11.cloned.1.call-update) | async-done | bytes 4194320 | tf_op jit(solution)/shard_map/all_gather | solution.py:26
  182.7 0.0 copy-done.2
  182.7 3.1 fusion.30
  185.9 2.5 collective-permute-start.1
  188.4 1.3 collective-permute-start.3
  189.7 0.0 copy-done.4
  189.7 0.1 slice_compare_fusion.1
  189.8 66.4 %all-gather.9.cloned.1.call-done = bf16[2,2048,512]{2,1,0:T(8,128)(2,1)} async-done(((bf16[2,256,512]{2,1,0:T(8,128)(2,1)}), bf16[2,2048,512]{2,1,0:T(8,128)(2,1)}) %all-gather.9.cloned.1.call-update) | async-done | bytes 4194320 | tf_op jit(solution)/shard_map/all_gather | solution.py:25
  256.1 75.1 %all-gather.15.cloned.1.call-done = bf16[2,512,2048]{2,1,0:T(8,128)(2,1)} async-done(((bf16[2,512,256]{2,1,0:T(8,128)(2,1)}), bf16[2,512,2048]{2,1,0:T(8,128)(2,1)}) %all-gather.15.cloned.1.call-update) | async-done | bytes 4194320 | tf_op jit(solution)/shard_map/all_gather | solution.py:29
  331.2 0.0 collective-permute-done.1
  331.2 0.0 collective-permute-done.3
  331.2 0.0 copy-start.1
  331.2 6.3 %convolution_convert_fusion.1 = bf16[512,2048]{1,0:T(8,128)(2,1)} fusion(bf16[2,512,2048]{2,1,0:T(8,128)(2,1)} %all-gather.15.cloned.1.call-done, bf16[2,2048,512]{2,1,0:T(8,128)(2,1)} %all-gather.9.cloned.1.call-done, bf16[512,512]{1,0:T(8,128)(2,1)S(1)} %fusion.30, bf16[1,512]{1,0:T(2,128)(2,1)S(1)} %collective-permute-done.3, ...), kind=kOutput, calls=%fused_computation.11 | convolution fusion | flops 2157969408 | bytes 8932352 | tf_op jit(solution)/shard_map/dot_general | solution.py:56
  337.5 0.0 reduce-scatter.3.cloned.1.call-update
  337.6 0.0 all-gather.17.cloned.1.call-start
  337.6 29.4 %reduce-scatter.3.cloned.1.call-done = bf16[512,512]{1,0:T(8,128)(2,1)} async-done(((bf16[512,2048]{1,0:T(8,128)(2,1)}), bf16[512,512]{1,0:T(8,128)(2,1)}) %reduce-scatter.3.cloned.1.call-update) | async-done | bytes 524304 | tf_op jit(solution)/shard_map/reduce_scatter | solution.py:57
  367.0 0.0 copy-done.1
  367.1 2.0 add_convert_fusion.1
  369.0 0.0 all-gather.17.cloned.1.call-update
  369.0 0.0 reduce-scatter.5.cloned.1.call-start
  369.1 22.7 %all-gather.17.cloned.1.call-done = bf16[512,2048]{1,0:T(8,128)(2,1)} async-done(((bf16[512,512]{1,0:T(8,128)(2,1)}), bf16[512,2048]{1,0:T(8,128)(2,1)}) %all-gather.17.cloned.1.call-update) | async-done | bytes 2097168 | tf_op jit(solution)/shard_map/all_gather | solution.py:32
  391.8 2.1 fusion.3
  393.8 0.0 copy-start.3
  393.8 0.0 copy-start.5
  393.9 3.7 fusion.27
  397.5 0.0 copy-done.3
  397.5 0.4 copy-done.5
  397.9 1.3 fusion.28
  399.2 3.4 collective-permute-start.4
  402.6 1.3 collective-permute-start.5
  403.9 0.0 collective-permute-done.4
  403.9 4.2 collective-permute-done.5
  408.1 0.0 copy-start
  408.1 6.3 %convolution_convert_fusion = bf16[512,2048]{1,0:T(8,128)(2,1)} fusion(bf16[2,512,2048]{2,1,0:T(8,128)(2,1)} %all-gather.15.cloned.1.call-done, bf16[2,2048,512]{2,1,0:T(8,128)(2,1)} %all-gather.9.cloned.1.call-done, bf16[512,512]{1,0:T(8,128)(2,1)S(1)} %fusion.28, bf16[1,512]{1,0:T(2,128)(2,1)S(1)} %collective-permute-done.5, ...), kind=kOutput, calls=%fused_computation.10 | convolution fusion | flops 2157969408 | bytes 8932352 | tf_op jit(solution)/shard_map/dot_general | solution.py:56
  414.4 0.0 reduce-scatter.5.cloned.1.call-update
  414.5 31.3 %reduce-scatter.5.cloned.1.call-done = bf16[512,512]{1,0:T(8,128)(2,1)} async-done(((bf16[512,2048]{1,0:T(8,128)(2,1)}), bf16[512,512]{1,0:T(8,128)(2,1)}) %reduce-scatter.5.cloned.1.call-update) | async-done | bytes 524304 | tf_op jit(solution)/shard_map/reduce_scatter | solution.py:57
  445.8 0.0 copy-done
  445.8 2.0 add_convert_fusion
  (4 shorter events, 0.0 us)
Async XLA Ops:
  6.5 27.7 %all-gather.7.cloned.1.call-start = ((), (), s32[]{:S(2)}) async-start(), calls=%async_computation.2 | async-start | bytes 2621440 | tf_op jit(solution)/shard_map/all_gather | solution.py:32
  7.3 101.9 %all-gather.13.cloned.1.call-start = ((), (), s32[]{:S(2)}) async-start(), calls=%async_computation.5 | async-start | bytes 4718592 | tf_op jit(solution)/shard_map/all_gather | solution.py:27
  8.0 174.7 %all-gather.11.cloned.1.call-start = ((), (), s32[]{:S(2)}) async-start(), calls=%async_computation.4 | async-start | bytes 4718592 | tf_op jit(solution)/shard_map/all_gather | solution.py:26
  8.7 247.4 %all-gather.9.cloned.1.call-start = ((), (), s32[]{:S(2)}) async-start(), calls=%async_computation.3 | async-start | bytes 4718592 | tf_op jit(solution)/shard_map/all_gather | solution.py:25
  9.3 321.9 %all-gather.15.cloned.1.call-start = ((), (), s32[]{:S(2)}) async-start(), calls=%async_computation.6 | async-start | bytes 4718592 | tf_op jit(solution)/shard_map/all_gather | solution.py:29
  9.9 357.1 %reduce-scatter.3.cloned.1.call-start = ((), (), s32[]{:S(2)}) async-start(), calls=%async_computation.7 | async-start | bytes 2621440 | tf_op jit(solution)/shard_map/reduce_scatter | solution.py:57
  11.3 8.3 %collective-permute-start = (s32[1]{0:T(128)}, s32[1]{0:T(128)}, u32[]{:S(2)}, u32[]{:S(2)}) collective-permute-start(s32[1]{0:T(128)} %get-tuple-element.21), channel_id=1, source_target_pairs={{0,4},{4,8},{8,12},{12,16},{16,20},{20,24},{24,28},{1,5},{5,9},{9,... | collective-permute-start | bytes 20 | tf_op jit(solution)/shard_map/ppermute | solution.py:16
  16.7 5.5 %collective-permute-start.2 = (s32[1]{0:T(128)}, s32[1]{0:T(128)}, u32[]{:S(2)}, u32[]{:S(2)}) collective-permute-start(s32[1]{0:T(128)} %get-tuple-element.22), channel_id=1, source_target_pairs={{4,0},{8,4},{12,8},{16,12},{20,16},{24,20},{28,24},{5,1},{9,5},{13... | collective-permute-start | bytes 20 | tf_op jit(solution)/shard_map/ppermute | solution.py:17
  109.2 73.5 %copy-start.2 = (bf16[512,2048]{1,0:T(8,128)(2,1)S(1)}, bf16[512,2048]{1,0:T(8,128)(2,1)}, u32[]{:S(2)}) copy-start(bf16[512,2048]{1,0:T(8,128)(2,1)} %all-gather.7.cloned.1.call-done) | copy-start | bytes 6291460
  113.9 75.8 %copy-start.4 = (s32[512]{0:T(512)S(1)}, s32[512]{0:T(512)}, u32[]{:S(2)}) copy-start(s32[512]{0:T(512)} %param.9) | copy-start | bytes 6148
  185.9 145.3 %collective-permute-start.1 = (bf16[1,512]{1,0:T(2,128)(2,1)S(1)}, bf16[1,512]{1,0:T(2,128)(2,1)S(1)}, u32[]{:S(2)}, u32[]{:S(2)}) collective-permute-start(bf16[1,512]{1,0:T(2,128)(2,1)S(1)} %get-tuple-element.7), channel_id=1, source_target_pairs={{0,4},{4,8},{8,12},{12,16},{16,20},{20,24},{24,28},{1,5},{5,9},{9,... | collective-permute-start | bytes 3080 | tf_op jit(solution)/shard_map/ppermute | solution.py:16
  188.4 142.8 %collective-permute-start.3 = (bf16[1,512]{1,0:T(2,128)(2,1)S(1)}, bf16[1,512]{1,0:T(2,128)(2,1)S(1)}, u32[]{:S(2)}, u32[]{:S(2)}) collective-permute-start(bf16[1,512]{1,0:T(2,128)(2,1)S(1)} %get-tuple-element.8), channel_id=1, source_target_pairs={{4,0},{8,4},{12,8},{16,12},{20,16},{24,20},{28,24},{5,1},{9,5},{13... | collective-permute-start | bytes 3080 | tf_op jit(solution)/shard_map/ppermute | solution.py:17
  331.2 35.8 %copy-start.1 = (bf16[512,512]{1,0:T(8,128)(2,1)S(1)}, bf16[512,512]{1,0:T(8,128)(2,1)}, u32[]{:S(2)}) copy-start(bf16[512,512]{1,0:T(8,128)(2,1)} %param.8) | copy-start | bytes 1572868
  337.6 54.2 %all-gather.17.cloned.1.call-start = ((), (), s32[]{:S(2)}) async-start(), calls=%async_computation.8 | async-start | bytes 2621440 | tf_op jit(solution)/shard_map/all_gather | solution.py:32
  369.0 76.7 %reduce-scatter.5.cloned.1.call-start = ((), (), s32[]{:S(2)}) async-start(), calls=%async_computation.9 | async-start | bytes 2621440 | tf_op jit(solution)/shard_map/reduce_scatter | solution.py:57
  393.8 3.7 copy-start.3
  393.8 4.1 copy-start.5
  399.2 4.7 %collective-permute-start.4 = (bf16[1,512]{1,0:T(2,128)(2,1)S(1)}, bf16[1,512]{1,0:T(2,128)(2,1)S(1)}, u32[]{:S(2)}, u32[]{:S(2)}) collective-permute-start(bf16[1,512]{1,0:T(2,128)(2,1)S(1)} %get-tuple-element.5), channel_id=1, source_target_pairs={{0,4},{4,8},{8,12},{12,16},{16,20},{20,24},{24,28},{1,5},{5,9},{9,... | collective-permute-start | bytes 3080 | tf_op jit(solution)/shard_map/ppermute | solution.py:16
  402.6 5.5 %collective-permute-start.5 = (bf16[1,512]{1,0:T(2,128)(2,1)S(1)}, bf16[1,512]{1,0:T(2,128)(2,1)S(1)}, u32[]{:S(2)}, u32[]{:S(2)}) collective-permute-start(bf16[1,512]{1,0:T(2,128)(2,1)S(1)} %get-tuple-element.6), channel_id=1, source_target_pairs={{4,0},{8,4},{12,8},{16,12},{20,16},{24,20},{28,24},{5,1},{9,5},{13... | collective-permute-start | bytes 3080 | tf_op jit(solution)/shard_map/ppermute | solution.py:17
  408.1 37.7 %copy-start = (bf16[512,512]{1,0:T(8,128)(2,1)S(1)}, bf16[512,512]{1,0:T(8,128)(2,1)}, u32[]{:S(2)}) copy-start(bf16[512,512]{1,0:T(8,128)(2,1)} %add_convert_fusion.1) | copy-start | bytes 1572868
Sparse Core Ops, SparseCore 0:
  8.9 25.2 all-gather.6
  36.4 72.7 all-gather.12
  111.4 71.2 all-gather.10
  184.8 71.2 all-gather.8
  258.0 73.1 all-gather.14
  337.7 29.3 reduce-scatter.2
  369.2 22.5 all-gather.16
  414.6 31.1 reduce-scatter.4
where the time goes:
time: 455 us
  waiting for transfers between devices  386 us (85%)
  matrix products  25.4 us (6%)
  starting transfers between devices  15.4 us (3%)
  between operations  13.6 us (3%)
  other arithmetic  10.3 us (2%)
    all_gather x1, waiting for transfers between devices, per_device(): gathered_out = lax.all_gather(out_proj, 'sp', axis=2, tiled=True)  75.1 us
    all_gather x1, waiting for transfers between devices, per_device(): lax.all_gather(value_proj, 'sp', axis=1, tiled=True)  72.9 us
    all_gather x1, waiting for transfers between devices, per_device(): lax.all_gather(input_gate, 'sp', axis=1, tiled=True)  68.9 us
    all_gather x1, waiting for transfers between devices, per_device(): lax.all_gather(gate_proj, 'sp', axis=1, tiled=True)  66.4 us
    reduce_scatter x2, waiting for transfers between devices, per_device(): lax.psum_scatter(partials.astype(jnp.bfloat16), 'tp', scatter_dimension=1...  60.7 us
    all_gather x2, waiting for transfers between devices, per_device(): full_rows = lax.all_gather(current, 'tp', axis=1, tiled=True)  32.6 us
    dot_general x2, matrix products, per_device(): jnp.dot(gated, gathered_out[layer_index], preferred_element_type=jnp.floa...  12.7 us
    ppermute x3, starting transfers between devices, with_halo(): before = lax.ppermute(last, axis, up)  11.2 us
  transfers between devices with their start and end apart: 14, of which 10 were waited for; matrix products, arithmetic and copies ran while one was open for 3% of the time, Pallas kernels for 0%

commit v1 on v0

--- a/solution.py
+++ b/solution.py
@@ -26,7 +26,7 @@
         lax.all_gather(input_gate, "sp", axis=1, tiled=True),
         lax.all_gather(value_proj, "sp", axis=1, tiled=True),
     )
-    gathered_out = lax.all_gather(out_proj, "sp", axis=2, tiled=True)
+    gathered_out = jnp.concatenate(lax.all_gather(out_proj, "sp"), axis=2)
     current = stream
     for layer_index in range(layers):
         full_rows = lax.all_gather(current, "tp", axis=1, tiled=True)

time: 455 us -> 454 us (level)
  waiting for transfers between devices: 386 us -> 378 us
  local copies, waits for them, and re-layouts: 3.38 us -> 10.9 us
    slice x0 -> x3, local copies, waits for them, and re-layouts: none -> 10.3 us  [per_device(): gathered_out[layer_index]]
    all_gather x1, waiting for transfers between devices: 75.1 us -> 66.4 us  [per_device(): gathered_out = jnp.concatenate(lax.all_gather(out_proj, 'sp'), axis=2)]
  transfers between devices with their start and end apart: 14 -> 14, of which waited for: 10 -> 10; matrix products, arithmetic and copies ran while one was open for 3% -> 5% of each run, Pallas kernels for 0% -> 0%
where the time goes in v1:
time: 454 us; the launch traced here: 453 us
  waiting for transfers between devices  378 us (83%)
  matrix products  25.1 us (6%)
  starting transfers between devices  15.4 us (3%)
  between operations  13.7 us (3%)
  local copies, waits for them, and re-layouts  10.9 us (2%)
  other arithmetic  9.91 us (2%)
    all_gather x1, waiting for transfers between devices, per_device(): lax.all_gather(value_proj, 'sp', axis=1, tiled=True)  72.8 us
    all_gather x1, waiting for transfers between devices, per_device(): lax.all_gather(input_gate, 'sp', axis=1, tiled=True)  69.6 us
    all_gather x1, waiting for transfers between devices, per_device(): gathered_out = jnp.concatenate(lax.all_gather(out_proj, 'sp'), axis=2)  66.4 us
    all_gather x1, waiting for transfers between devices, per_device(): lax.all_gather(gate_proj, 'sp', axis=1, tiled=True)  65.5 us
    reduce_scatter x2, waiting for transfers between devices, per_device(): lax.psum_scatter(partials.astype(jnp.bfloat16), 'tp', scatter_dimension=1...  61.1 us
    all_gather x2, waiting for transfers between devices, per_device(): full_rows = lax.all_gather(current, 'tp', axis=1, tiled=True)  33.7 us
    dot_general x2, matrix products, per_device(): jnp.dot(gated, gathered_out[layer_index], preferred_element_type=jnp.floa...  13.7 us
    ppermute x3, starting transfers between devices, with_halo(): before = lax.ppermute(last, axis, up)  11.3 us
  transfers between devices with their start and end apart: 14, of which 10 were waited for; matrix products, arithmetic and copies ran while one was open for 5% of the time, Pallas kernels for 0%

profile of v1, /device:TPU:0, one launch (start us, length us, event | category | flops | bytes accessed | tf_op | source)
XLA Modules:
  0.0 453.4 jit_solution(7753369005543131244)
XLA Ops:
  6.5 0.0 copy-start.5
  6.5 0.0 copy-start.6
  6.5 0.0 all-gather.8.cloned.1.call-start
  6.5 0.7 all-gather.8.cloned.1.call-update
  7.3 0.0 all-gather.14.cloned.1.call-start
  7.3 0.7 all-gather.14.cloned.1.call-update
  8.0 0.0 all-gather.12.cloned.1.call-start
  8.1 0.7 all-gather.12.cloned.1.call-update
  8.7 0.0 all-gather.18.cloned.1.call-start
  8.8 0.5 all-gather.18.cloned.1.call-update
  9.3 0.0 all-gather.10.cloned.1.call-start
  9.4 0.5 all-gather.10.cloned.1.call-update
  9.9 0.0 reduce-scatter.3.cloned.1.call-start
  10.0 0.0 copy-done.5
  10.0 0.6 fusion.65
  10.6 5.5 %collective-permute-start = (s32[1]{0:T(128)}, s32[1]{0:T(128)}, u32[]{:S(2)}, u32[]{:S(2)}) collective-permute-start(s32[1]{0:T(128)} %get-tuple-element.23), channel_id=1, source_target_pairs={{0,4},{4,8},{8,12},{12,16},{16,20},{20,24},{24,28},{1,5},{5,9},{9,... | collective-permute-start | bytes 20 | tf_op jit(solution)/shard_map/ppermute | solution.py:16
  16.0 1.3 collective-permute-start.2
  17.3 0.0 copy-done.6
  17.3 0.0 copy-done.4
  17.4 0.0 collective-permute-done
  17.4 4.3 collective-permute-done.2
  21.6 1.4 pad_add_fusion
  23.1 0.1 slice_compare_fusion.1
  23.2 11.1 %all-gather.8.cloned.1.call-done = bf16[512,2048]{1,0:T(8,128)(2,1)} async-done(((bf16[512,512]{1,0:T(8,128)(2,1)}), bf16[512,2048]{1,0:T(8,128)(2,1)}) %all-gather.8.cloned.1.call-update) | async-done | bytes 2097168 | tf_op jit(solution)/shard_map/all_gather | solution.py:32
  34.2 0.0 copy-start.2
  34.2 2.2 fusion
  36.5 72.8 %all-gather.14.cloned.1.call-done = bf16[2,2048,512]{2,1,0:T(8,128)(2,1)} async-done(((bf16[2,256,512]{2,1,0:T(8,128)(2,1)}), bf16[2,2048,512]{2,1,0:T(8,128)(2,1)}) %all-gather.14.cloned.1.call-update) | async-done | bytes 4194320 | tf_op jit(solution)/shard_map/all_gather | solution.py:27
  109.2 0.0 copy-done.2
  109.2 3.9 fusion.19
  113.1 69.6 %all-gather.12.cloned.1.call-done = bf16[2,2048,512]{2,1,0:T(8,128)(2,1)} async-done(((bf16[2,256,512]{2,1,0:T(8,128)(2,1)}), bf16[2,2048,512]{2,1,0:T(8,128)(2,1)}) %all-gather.12.cloned.1.call-update) | async-done | bytes 4194320 | tf_op jit(solution)/shard_map/all_gather | solution.py:26
  182.7 3.2 fusion.30
  185.9 2.4 collective-permute-start.1
  188.4 1.3 collective-permute-start.3
  189.7 66.4 %all-gather.18.cloned.1.call-done = bf16[16,512,256]{2,1,0:T(8,128)(2,1)} async-done(((bf16[2,512,256]{2,1,0:T(8,128)(2,1)}), bf16[16,512,256]{2,1,0:T(8,128)(2,1)}) %all-gather.18.cloned.1.call-update) | async-done | bytes 4194320 | tf_op jit(solution)/shard_map/all_gather | solution.py:29
  256.1 3.9 fusion.60
  260.0 3.9 copy.11
  263.9 65.5 %all-gather.10.cloned.1.call-done = bf16[2,2048,512]{2,1,0:T(8,128)(2,1)} async-done(((bf16[2,256,512]{2,1,0:T(8,128)(2,1)}), bf16[2,2048,512]{2,1,0:T(8,128)(2,1)}) %all-gather.10.cloned.1.call-update) | async-done | bytes 4194320 | tf_op jit(solution)/shard_map/all_gather | solution.py:25
  329.5 0.0 collective-permute-done.1
  329.5 0.0 collective-permute-done.3
  329.5 6.8 %convolution_convert_fusion.1 = bf16[512,2048]{1,0:T(8,128)(2,1)} fusion(bf16[512,2048]{0,1:T(8,128)(2,1)} %bitcast.78, bf16[2,2048,512]{2,1,0:T(8,128)(2,1)} %all-gather.10.cloned.1.call-done, bf16[512,512]{1,0:T(8,128)(2,1)S(1)} %fusion.30, bf16[1,512]{1,0:T(2,128)(2,1)S(1)} %collective-permute-done.3, bf16[1,512]{1,0:T(2,128)(2,1)S(1)} %collective-permute-done.1, ...), kind=kOutput, calls=%fused_computation.11 | convolution fusion | flops 2157969408 | bytes 8932352 | tf_op jit(solution)/shard_map/dot_general | solution.py:56
  336.3 0.0 reduce-scatter.3.cloned.1.call-update
  336.3 0.0 all-gather.16.cloned.1.call-start
  336.4 29.8 %reduce-scatter.3.cloned.1.call-done = bf16[512,512]{1,0:T(8,128)(2,1)} async-done(((bf16[512,2048]{1,0:T(8,128)(2,1)}), bf16[512,512]{1,0:T(8,128)(2,1)}) %reduce-scatter.3.cloned.1.call-update) | async-done | bytes 524304 | tf_op jit(solution)/shard_map/reduce_scatter | solution.py:57
  366.2 0.0 copy-done.1
  366.2 2.0 add_convert_fusion.1
  368.2 0.0 all-gather.16.cloned.1.call-update
  368.2 0.0 reduce-scatter.5.cloned.1.call-start
  368.2 22.7 %all-gather.16.cloned.1.call-done = bf16[512,2048]{1,0:T(8,128)(2,1)} async-done(((bf16[512,512]{1,0:T(8,128)(2,1)}), bf16[512,2048]{1,0:T(8,128)(2,1)}) %all-gather.16.cloned.1.call-update) | async-done | bytes 2097168 | tf_op jit(solution)/shard_map/all_gather | solution.py:32
  390.9 2.2 fusion.3
  393.1 0.0 copy-done.3
  393.1 0.0 copy-start.7
  393.1 3.0 fusion.27
  396.2 0.0 copy-done.7
  396.2 1.3 fusion.28
  397.5 3.4 collective-permute-start.4
  400.9 1.3 collective-permute-start.5
  402.2 2.5 copy.12
  404.6 0.0 collective-permute-done.4
  404.6 1.7 collective-permute-done.5
  406.4 6.9 %convolution_convert_fusion = bf16[512,2048]{1,0:T(8,128)(2,1)} fusion(bf16[512,2048]{0,1:T(8,128)(2,1)} %bitcast.79, bf16[2,2048,512]{2,1,0:T(8,128)(2,1)} %all-gather.10.cloned.1.call-done, bf16[512,512]{1,0:T(8,128)(2,1)S(1)} %fusion.28, bf16[1,512]{1,0:T(2,128)(2,1)S(1)} %collective-permute-done.5, bf16[1,512]{1,0:T(2,128)(2,1)S(1)} %collective-permute-done.4, ...), kind=kOutput, calls=%fused_computation.10 | convolution fusion | flops 2157969408 | bytes 8932352 | tf_op jit(solution)/shard_map/dot_general | solution.py:56
  413.3 0.0 reduce-scatter.5.cloned.1.call-update
  413.3 31.3 %reduce-scatter.5.cloned.1.call-done = bf16[512,512]{1,0:T(8,128)(2,1)} async-done(((bf16[512,2048]{1,0:T(8,128)(2,1)}), bf16[512,512]{1,0:T(8,128)(2,1)}) %reduce-scatter.5.cloned.1.call-update) | async-done | bytes 524304 | tf_op jit(solution)/shard_map/reduce_scatter | solution.py:57
  444.6 0.0 copy-done
  444.6 2.0 add_convert_fusion
  (10 shorter events, 0.1 us)
Async XLA Ops:
  6.5 3.4 copy-start.5
  6.5 10.8 %copy-start.6 = (f32[2,3,512]{2,0,1:T(2,128)S(1)}, f32[2,3,512]{2,0,1:T(2,128)}, u32[]{:S(2)}) copy-start(f32[2,3,512]{2,0,1:T(2,128)} %param.14) | copy-start | bytes 36868
  6.5 10.8 %copy-start.4 = (f32[2,2048]{1,0:T(2,128)S(1)}, f32[2,2048]{1,0:T(2,128)}, u32[]{:S(2)}) copy-start(f32[2,2048]{1,0:T(2,128)} %param.10) | copy-start | bytes 49156
  6.5 27.7 %all-gather.8.cloned.1.call-start = ((), (), s32[]{:S(2)}) async-start(), calls=%async_computation.2 | async-start | bytes 2621440 | tf_op jit(solution)/shard_map/all_gather | solution.py:32
  7.3 101.9 %all-gather.14.cloned.1.call-start = ((), (), s32[]{:S(2)}) async-start(), calls=%async_computation.5 | async-start | bytes 4718592 | tf_op jit(solution)/shard_map/all_gather | solution.py:27
  8.0 174.7 %all-gather.12.cloned.1.call-start = ((), (), s32[]{:S(2)}) async-start(), calls=%async_computation.4 | async-start | bytes 4718592 | tf_op jit(solution)/shard_map/all_gather | solution.py:26
  8.7 247.3 %all-gather.18.cloned.1.call-start = ((), (), s32[]{:S(2)}) async-start(), calls=%async_computation.9 | async-start | bytes 4718592 | tf_op jit(solution)/shard_map/all_gather | solution.py:29
  9.3 320.1 %all-gather.10.cloned.1.call-start = ((), (), s32[]{:S(2)}) async-start(), calls=%async_computation.3 | async-start | bytes 4718592 | tf_op jit(solution)/shard_map/all_gather | solution.py:25
  9.9 356.3 %reduce-scatter.3.cloned.1.call-start = ((), (), s32[]{:S(2)}) async-start(), calls=%async_computation.6 | async-start | bytes 2621440 | tf_op jit(solution)/shard_map/reduce_scatter | solution.py:57
  10.6 6.8 %collective-permute-start = (s32[1]{0:T(128)}, s32[1]{0:T(128)}, u32[]{:S(2)}, u32[]{:S(2)}) collective-permute-start(s32[1]{0:T(128)} %get-tuple-element.23), channel_id=1, source_target_pairs={{0,4},{4,8},{8,12},{12,16},{16,20},{20,24},{24,28},{1,5},{5,9},{9,... | collective-permute-start | bytes 20 | tf_op jit(solution)/shard_map/ppermute | solution.py:16
  16.0 5.6 %collective-permute-start.2 = (s32[1]{0:T(128)}, s32[1]{0:T(128)}, u32[]{:S(2)}, u32[]{:S(2)}) collective-permute-start(s32[1]{0:T(128)} %get-tuple-element.24), channel_id=1, source_target_pairs={{4,0},{8,4},{12,8},{16,12},{20,16},{24,20},{28,24},{5,1},{9,5},{13... | collective-permute-start | bytes 20 | tf_op jit(solution)/shard_map/ppermute | solution.py:17
  34.2 75.0 %copy-start.2 = (bf16[512,2048]{1,0:T(8,128)(2,1)S(1)}, bf16[512,2048]{1,0:T(8,128)(2,1)}, u32[]{:S(2)}) copy-start(bf16[512,2048]{1,0:T(8,128)(2,1)} %all-gather.8.cloned.1.call-done) | copy-start | bytes 6291460
  185.9 143.5 %collective-permute-start.1 = (bf16[1,512]{1,0:T(2,128)(2,1)S(1)}, bf16[1,512]{1,0:T(2,128)(2,1)S(1)}, u32[]{:S(2)}, u32[]{:S(2)}) collective-permute-start(bf16[1,512]{1,0:T(2,128)(2,1)S(1)} %get-tuple-element.9), channel_id=1, source_target_pairs={{0,4},{4,8},{8,12},{12,16},{16,20},{20,24},{24,28},{1,5},{5,9},{9,... | collective-permute-start | bytes 3080 | tf_op jit(solution)/shard_map/ppermute | solution.py:16
  188.4 141.1 %collective-permute-start.3 = (bf16[1,512]{1,0:T(2,128)(2,1)S(1)}, bf16[1,512]{1,0:T(2,128)(2,1)S(1)}, u32[]{:S(2)}, u32[]{:S(2)}) collective-permute-start(bf16[1,512]{1,0:T(2,128)(2,1)S(1)} %get-tuple-element.10), channel_id=1, source_target_pairs={{4,0},{8,4},{12,8},{16,12},{20,16},{24,20},{28,24},{5,1},{9,5},{13... | collective-permute-start | bytes 3080 | tf_op jit(solution)/shard_map/ppermute | solution.py:17
  336.3 29.9 %copy-start.1 = (bf16[512,512]{1,0:T(8,128)(2,1)S(1)}, bf16[512,512]{1,0:T(8,128)(2,1)}, u32[]{:S(2)}) copy-start(bf16[512,512]{1,0:T(8,128)(2,1)} %param.8) | copy-start | bytes 1572868
  336.3 54.6 %all-gather.16.cloned.1.call-start = ((), (), s32[]{:S(2)}) async-start(), calls=%async_computation.7 | async-start | bytes 2621440 | tf_op jit(solution)/shard_map/all_gather | solution.py:32
  368.2 76.4 %reduce-scatter.5.cloned.1.call-start = ((), (), s32[]{:S(2)}) async-start(), calls=%async_computation.8 | async-start | bytes 2621440 | tf_op jit(solution)/shard_map/reduce_scatter | solution.py:57
  390.9 2.2 copy-start.3
  393.1 3.1 copy-start.7
  397.5 7.1 %collective-permute-start.4 = (bf16[1,512]{1,0:T(2,128)(2,1)S(1)}, bf16[1,512]{1,0:T(2,128)(2,1)S(1)}, u32[]{:S(2)}, u32[]{:S(2)}) collective-permute-start(bf16[1,512]{1,0:T(2,128)(2,1)S(1)} %get-tuple-element.7), channel_id=1, source_target_pairs={{0,4},{4,8},{8,12},{12,16},{16,20},{20,24},{24,28},{1,5},{5,9},{9,... | collective-permute-start | bytes 3080 | tf_op jit(solution)/shard_map/ppermute | solution.py:16
  400.9 5.5 %collective-permute-start.5 = (bf16[1,512]{1,0:T(2,128)(2,1)S(1)}, bf16[1,512]{1,0:T(2,128)(2,1)S(1)}, u32[]{:S(2)}, u32[]{:S(2)}) collective-permute-start(bf16[1,512]{1,0:T(2,128)(2,1)S(1)} %get-tuple-element.8), channel_id=1, source_target_pairs={{4,0},{8,4},{12,8},{16,12},{20,16},{24,20},{28,24},{5,1},{9,5},{13... | collective-permute-start | bytes 3080 | tf_op jit(solution)/shard_map/ppermute | solution.py:17
  413.3 31.3 %copy-start = (bf16[512,512]{1,0:T(8,128)(2,1)S(1)}, bf16[512,512]{1,0:T(8,128)(2,1)}, u32[]{:S(2)}) copy-start(bf16[512,512]{1,0:T(8,128)(2,1)} %add_convert_fusion.1) | copy-start | bytes 1572868
Sparse Core Ops, SparseCore 0:
  8.9 25.2 all-gather.7
  36.4 72.7 all-gather.13
  111.4 71.2 all-gather.11
  184.7 71.3 all-gather.17
  258.1 71.2 all-gather.9
  336.4 29.7 reduce-scatter.2
  368.3 22.5 all-gather.15
  413.4 31.1 reduce-scatter.4
